TPU v7x, 32 devices: a whole 2x2x4 slice. The times are simulated.
32 devices in a mesh: sp: 4 (over y, x), tp: 8 (over z, core).
Axes of the slice: x: 2, y: 2, z: 4, core: 2. Of those that a mesh axis runs over, the one named last changes fastest.
Arguments:
- tokens: bfloat16 [2, 512, 4096], P(None, 'sp', 'tp'), may hold values from -6 to 6
- key_matrix: bfloat16 [4096, 4096], P(None, 'tp'), may hold values from -0.09375 to 0.09375
- value_matrix: bfloat16 [4096, 4096], P(None, 'tp'), may hold values from -0.375 to 0.375
- gate_matrix: bfloat16 [4096, 64], replicated, may hold values from -0.09375 to 0.09375
- head_decay_rate: float32 [32], P('tp'), may hold values from 0 to 1, as said below
- extra_log_decay: float32 [2, 32, 512], P(None, 'tp', 'sp'), may hold values from -3 to 0, as said below
- next_token_query: bfloat16 [2, 4096], P(None, 'tp'), may hold values from -6 to 6
- next_token_key: bfloat16 [2, 4096], P(None, 'tp'), may hold values from -6 to 6
- next_token_value: bfloat16 [2, 32, 128], P(None, 'tp', 'sp'), may hold values from -6 to 6
- next_write_strength: float32 [2, 32], P(None, 'tp'), may hold values from 0.05 to 1
- read_norm_gain: float32 [128], P('sp'), may hold values from 0.1 to 1.9
Outputs:
- state_cache: bfloat16 [2, 32, 128, 128], P(None, 'tp', None, 'sp')
- first_read: bfloat16 [2, 32, 128], P(None, 'tp', 'sp')
Inputs may be any that keep to these rules, and one draw needn't show every extreme that they name: `head_decay_rate`: positive. `extra_log_decay`: never positive.
All inputs are finite; a program needn't handle non-finite values.
Results may differ from a plain program's by a relative error of at most 0.013.
Values may be sent and summed in bfloat16 or wider, within the bound.
A program may use at most 64 MiB of HBM per device.

v0:
```python
import jax
import jax.numpy as jnp
from jax import lax
from jax.sharding import PartitionSpec as P

DV = 128
exact_mode = lax.Precision.HIGHEST
strength_offset = 5.0


def unit_rows(matrix):
    return matrix * lax.rsqrt(jnp.sum(matrix * matrix, axis=-1, keepdims=True) + 1e-06)


def nilpotent_inverse(mixing):
    extent = mixing.shape[-1]
    result = jnp.zeros_like(mixing) + jnp.eye(extent, dtype=jnp.float32)
    powered = -mixing
    covered = 1
    while covered < extent:
        product = lax.optimization_barrier(
            jnp.einsum("...ij,...jk->...ik", result, powered, precision=exact_mode)
        )
        result = result + product
        powered = jnp.einsum("...ij,...jk->...ik", powered, powered, precision=exact_mode)
        covered = covered * 2
    return result


def block_terms(unit_keys, values, decay_logarithm, strength):
    extent = unit_keys.shape[-2]
    lower = jnp.tril(jnp.ones((extent, extent), jnp.bool_))
    strict = jnp.tril(jnp.ones((extent, extent), jnp.bool_), -1)
    running = jnp.cumsum(decay_logarithm, axis=-1)
    spread = running[..., :, None] - running[..., None, :]
    within = jnp.where(lower, jnp.exp(jnp.where(lower, spread, 0.0)), 0.0)
    scaled = unit_keys * strength[..., None]
    mixing = jnp.where(
        strict,
        jnp.einsum("...id,...jd->...ij", scaled, unit_keys, precision=exact_mode) * within,
        0.0,
    )
    inverse = nilpotent_inverse(mixing)
    writes = jnp.einsum(
        "...ij,...je->...ie", inverse, values * strength[..., None], precision=exact_mode
    )
    erases = jnp.einsum(
        "...ij,...jd->...id", inverse, scaled * jnp.exp(running)[..., None], precision=exact_mode
    )
    final_log = running[..., -1]
    carried = unit_keys * jnp.exp(final_log[..., None] - running)[..., None]
    return (writes, erases, carried, final_log)


def split_blocks(array, block_count):
    shaped = array.reshape(
        array.shape[:2] + (block_count, array.shape[2] // block_count) + array.shape[3:]
    )
    return jnp.moveaxis(shaped, 2, 0)


def local(
    tokens,
    key_matrix,
    value_matrix,
    gate_matrix,
    head_decay_rate,
    extra_log_decay,
    next_token_query,
    next_token_key,
    next_token_value,
    next_write_strength,
    read_norm_gain,
):
    sequences, positions, _ = tokens.shape
    local_heads = head_decay_rate.shape[0]
    key_width = key_matrix.shape[1] // local_heads
    value_width = value_matrix.shape[1] // local_heads
    all_heads = gate_matrix.shape[1] // 2
    group_size = lax.axis_size("sp")
    column_share = value_width // group_size
    first_head = lax.axis_index("tp") * local_heads
    decay_cols = lax.dynamic_slice_in_dim(gate_matrix, first_head, local_heads, 1)
    strength_cols = lax.dynamic_slice_in_dim(gate_matrix, all_heads + first_head, local_heads, 1)
    gate_cols = jnp.concatenate([decay_cols, strength_cols], axis=1)
    row_count = sequences * positions
    incoming = lax.all_gather(tokens, "tp", axis=2, tiled=True)
    span_width = incoming.shape[2]
    flat_rows = incoming.reshape(row_count, span_width)
    products = lax.optimization_barrier(
        (
            jnp.dot(flat_rows, key_matrix, preferred_element_type=jnp.float32),
            jnp.dot(flat_rows, value_matrix, preferred_element_type=jnp.float32),
            jnp.dot(flat_rows, gate_cols, preferred_element_type=jnp.float32),
        )
    )
    key_sum = products[0]
    value_sum = products[1]
    gate_pre = products[2]
    key_float = lax.optimization_barrier(key_sum.astype(jnp.bfloat16)).astype(jnp.float32)
    value_float = lax.optimization_barrier(value_sum.astype(jnp.bfloat16)).astype(jnp.float32)
    unit_keys = unit_rows(
        key_float.reshape(sequences, positions, local_heads, key_width).transpose(0, 2, 1, 3)
    )
    values = value_float.reshape(sequences, positions, local_heads, value_width).transpose(
        0, 2, 1, 3
    )
    gate_projected = gate_pre.reshape(sequences, positions, 2 * local_heads).transpose(0, 2, 1)
    decay_logarithm = (
        -head_decay_rate[None, :, None] * jax.nn.softplus(gate_projected[:, :local_heads])
        + extra_log_decay
    )
    strength = jax.nn.sigmoid(gate_projected[:, local_heads:] - strength_offset)
    block_count = positions // min(64, positions)
    block_parts = block_terms(
        split_blocks(unit_keys, block_count),
        split_blocks(values, block_count),
        split_blocks(decay_logarithm, block_count),
        split_blocks(strength, block_count),
    )
    identity = jnp.zeros((sequences, local_heads, key_width, key_width), jnp.float32) + jnp.eye(
        key_width, dtype=jnp.float32
    )
    start_map = jnp.concatenate(
        [identity, jnp.zeros((sequences, local_heads, key_width, value_width), jnp.float32)],
        axis=-1,
    )

    def advance(current, block_part):
        writes, erases, carried, final_log = block_part
        padded = jnp.concatenate(
            [jnp.zeros(writes.shape[:-1] + (key_width,), jnp.float32), writes], axis=-1
        )
        removed = lax.optimization_barrier(
            jnp.einsum("shcd,shde->shce", erases, current, precision=exact_mode)
        )
        fresh = padded - removed
        added = lax.optimization_barrier(
            jnp.einsum("shcd,shce->shde", carried, fresh, precision=exact_mode)
        )
        current = current * jnp.exp(final_log)[..., None, None] + added
        return (current, None)

    local_map, _ = lax.scan(advance, start_map, block_parts)
    carry_map = local_map[..., :key_width]
    write_map = local_map[..., key_width:]
    carry_copies = jnp.broadcast_to(carry_map[None], (group_size,) + carry_map.shape)
    write_parts = jnp.moveaxis(
        write_map.reshape(sequences, local_heads, key_width, group_size, column_share), 3, 0
    )
    carries = lax.all_to_all(carry_copies, "sp", split_axis=0, concat_axis=0, tiled=True)
    write_cols = lax.all_to_all(write_parts, "sp", split_axis=0, concat_axis=0, tiled=True)

    def fold_step(current, block_map):
        moved = lax.optimization_barrier(
            jnp.einsum("shij,shje->shie", block_map[0], current, precision=exact_mode)
        )
        return (moved + block_map[1], None)

    begin_state = jnp.zeros(write_cols.shape[1:], jnp.float32)
    folded, _ = lax.scan(fold_step, begin_state, (carries, write_cols))
    query_rows = next_token_query.astype(jnp.float32).reshape(sequences, local_heads, key_width)
    unit_new = unit_rows(
        next_token_key.astype(jnp.float32).reshape(sequences, local_heads, key_width)
    )
    value_rows = next_token_value.astype(jnp.float32)
    key_read = jnp.einsum("shd,shde->she", unit_new, folded, precision=exact_mode)
    query_read = jnp.einsum("shd,shde->she", query_rows, folded, precision=exact_mode)
    intersection = jnp.sum(query_rows * unit_new, axis=-1)
    read_raw = query_read + (next_write_strength * intersection)[..., None] * (
        value_rows - key_read
    )
    square_total = lax.psum(jnp.sum(read_raw * read_raw, axis=-1, keepdims=True), "sp")
    first_read = read_raw * lax.rsqrt(square_total / DV + 1e-06) * read_norm_gain
    return (folded.astype(jnp.bfloat16), first_read.astype(jnp.bfloat16))


def solution(mesh):
    in_specs = (
        P(None, "sp", "tp"),
        P(None, "tp"),
        P(None, "tp"),
        P(),
        P("tp"),
        P(None, "tp", "sp"),
        P(None, "tp"),
        P(None, "tp"),
        P(None, "tp", "sp"),
        P(None, "tp"),
        P("sp"),
    )
    out_specs = (P(None, "tp", None, "sp"), P(None, "tp", "sp"))
    return jax.shard_map(local, mesh=mesh, in_specs=in_specs, out_specs=out_specs, check_vma=False)
```

profile of v0, /device:TPU:0, one launch (start us, length us, event | category | flops | bytes accessed | tf_op | source)
XLA Modules:
  0.0 130.1 jit_solution(6070156353231956708)
XLA Ops:
  7.2 0.7 all-gather.2.cloned.1.call-update
  7.9 0.7 neg.14
  8.6 0.1 concatenate.9
  8.7 0.1 iota_compare_fusion.1
  8.8 0.9 constant_dynamic-slice_fusion.2
  9.7 31.8 %all-gather.2.cloned.1.call-done = bf16[2,128,4096]{2,1,0:T(8,128)(2,1)} async-done(((bf16[2,128,512]{2,1,0:T(8,128)(2,1)}), bf16[2,128,4096]{2,1,0:T(8,128)(2,1)}) %all-gather.2.cloned.1.call-update) | async-done | bytes 2097168 | tf_op jit(solution)/shard_map/all_gather | solution.py:87
  41.5 4.2 %fusion.52 = bf16[256,512]{1,0:T(8,128)(2,1)S(1)} fusion(bf16[256,4096]{1,0:T(8,128)(2,1)} %bitcast.96, bf16[4096,512]{1,0:T(8,128)(2,1)} %param.16), kind=kOutput, calls=%fused_computation.86 | convolution fusion | flops 1073741824 | bytes 6553600 | tf_op jit(solution)/shard_map/dot_general | solution.py:92
  45.7 0.4 copy-done.7
  46.2 1.2 fusion.53
  47.4 0.6 convolution_bitcast_fusion
  48.1 0.1 fusion.49
  48.2 0.1 reshape.99
  48.2 1.1 reduce_window_sum.11
  49.3 0.2 slice_reduce_fusion
  49.5 0.1 fusion.51
  49.6 0.2 reshape.112
  49.8 0.2 fusion.23
  50.0 0.2 bitcast_multiply_fusion
  50.2 0.1 reshape.102
  50.3 0.2 reshape.114
  50.5 0.5 broadcast_multiply_fusion
  51.0 1.0 fusion.22
  52.0 0.6 fusion.54
  52.6 0.6 fusion.33
  53.2 0.6 fusion.55
  53.9 0.7 fusion.30
  54.6 0.6 fusion.56
  55.2 0.7 fusion.38
  55.9 0.1 fusion.37
  56.0 0.6 fusion.58
  56.7 0.6 fusion.57
  57.4 0.6 fusion.60
  58.0 0.7 fusion.59
  58.7 0.1 add.116
  58.8 0.7 fusion.61
  59.5 0.7 fusion.24
  60.1 0.7 fusion.26
  60.8 4.5 %while.21 = (s32[]{:T(128)}, f32[2,4,128,256]{3,2,1,0:T(8,128)S(1)}, f32[2,2,4]{2,1,0:T(2,128)S(1)}, f32[2,2,4,64,128]{4,3,0,2,1:T(8,128)S(1)}, f32[2,2,4,64,128...) while((s32[]{:T(128)}, f32[2,4,128,256]{3,2,1,0:T(8,128)S(1)}, ...), condition=%wide.region_3.4_spmd, body=%wide.region_2.3_spmd.sunk | while | flops 403308544 | bytes 7602365 | solution.py:144
  61.0 0.7 fusion.107
  61.8 1.1 fusion.108
  62.9 0.3 multiply_add_fusion.3
  63.2 0.7 fusion.107
  64.0 1.1 fusion.108
  65.0 0.3 multiply_add_fusion.3
  65.4 0.3 copy.37
  65.7 0.8 copy.38
  66.6 3.6 %all-to-all-start.1 = ((f32[4,2,4,128,32]{3,4,2,1,0:T(8,128)}), f32[4,2,4,128,32]{3,4,2,1,0:T(8,128)S(1)}, u32[]{:S(2)}, u32[]{:S(2)}) async-start(f32[4,2,4,128,32]{3,4,2,1,0:T(8,128)} %copy.38), calls=%async_computation.1 | async-start | bytes 1048576 | tf_op jit(solution)/shard_map/all_to_all | solution.py:152
  70.3 8.5 %all-to-all-done.1 = f32[4,2,4,128,32]{3,4,2,1,0:T(8,128)S(1)} async-done(((f32[4,2,4,128,32]{3,4,2,1,0:T(8,128)}), f32[4,2,4,128,32]{3,4,2,1,0:T(8,128)S(1)}, u32[]{:S(2)}, u32[]{:S(2)}) %all-to-all-start.1) | async-done | bytes 524320 | tf_op jit(solution)/shard_map/all_to_all | solution.py:152
  78.7 1.6 %broadcast_in_dim.51 = f32[4,2,4,128,128]{4,3,2,1,0:T(8,128)} broadcast(f32[2,4,128,128]{3,2,1,0:T(8,128)S(1)} %slice.18), dimensions={1,2,3,4} | broadcast | bytes 2621440 | tf_op jit(solution)/shard_map/broadcast_in_dim | solution.py:147
  80.3 3.7 %all-to-all-start = ((f32[4,2,4,128,128]{4,3,2,1,0:T(8,128)}), f32[4,2,4,128,128]{4,3,2,1,0:T(8,128)S(1)}, u32[]{:S(2)}, u32[]{:S(2)}) async-start(f32[4,2,4,128,128]{4,3,2,1,0:T(8,128)} %broadcast_in_dim.51), calls=%async_computation | async-start | bytes 4194304 | tf_op jit(solution)/shard_map/all_to_all | solution.py:151
  84.1 0.1 multiply_reduce_fusion.2
  84.2 0.2 multiply_reduce_fusion.1
  84.4 24.1 %all-to-all-done = f32[4,2,4,128,128]{4,3,2,1,0:T(8,128)S(1)} async-done(((f32[4,2,4,128,128]{4,3,2,1,0:T(8,128)}), f32[4,2,4,128,128]{4,3,2,1,0:T(8,128)S(1)}, u32[]{:S(2)}, u32[]{:S(2)}) %all-to-all-start) | async-done | bytes 2097184 | tf_op jit(solution)/shard_map/all_to_all | solution.py:151
  108.5 3.9 %while.22 = (s32[]{:T(128)}, f32[2,4,128,32]{2,3,1,0:T(8,128)S(1)}, f32[4,2,4,128,128]{4,3,2,1,0:T(8,128)S(1)}, f32[4,2,4,128,32]{3,4,2,1,0:T(8,128)S(1)}, s32[]{:T(128)}, /*index=5*/s32[]{:T(128)}) while((s32[]{:T(128)}, f32[2,4,128,32]{2,3,1,0:T(8,128)S(1)}, f32[4,2,4,128,128]{4,3,2,1,0:T(8,128)S(1)}, ...), condition=%wide.region_5.6_spmd.clone, body=%wide.region_4.5_spmd.clone.sunk | while | flops 50397184 | bytes 1179735 | solution.py:161
  108.5 0.9 fusion.112
  109.5 0.9 fusion.112
  110.4 0.9 fusion.112
  111.4 0.9 fusion.112
  112.4 0.6 convert_element_type.39
  113.0 0.3 fusion.63
  113.3 0.2 fusion.62
  113.6 0.2 multiply_reduce_fusion
  113.7 8.9 %psum.7 = f32[2,4,1]{1,0,2:T(2,128)S(1)} all-reduce(f32[2,4,1]{1,0,2:T(2,128)S(1)} %bitcast.111), channel_id=1, replica_groups=mesh['sp'=4,'tp'=8] {'sp'}, use_global_device_ids=true, to_apply=%region_9.10 | all-reduce | flops 8 | bytes 64 | tf_op jit(solution)/shard_map/psum | solution.py:173
  122.6 0.7 multiply_convert_fusion
  (43 shorter events, 0.6 us)
Async XLA Ops:
  7.2 34.3 %all-gather.2.cloned.1.call-start = ((), (), s32[]{:S(2)}) async-start(), calls=%async_computation.2 | async-start | bytes 2359296 | tf_op jit(solution)/shard_map/all_gather | solution.py:87
  41.5 4.2 %copy-start = (bf16[2,128,4096]{2,1,0:T(8,128)(2,1)S(1)}, bf16[2,128,4096]{2,1,0:T(8,128)(2,1)}, u32[]{:S(2)}) copy-start(bf16[2,128,4096]{2,1,0:T(8,128)(2,1)} %all-gather.2.cloned.1.call-done) | copy-start | bytes 6291460
  41.5 4.7 %copy-start.7 = (bf16[4096,512]{1,0:T(8,128)(2,1)S(1)}, bf16[4096,512]{1,0:T(8,128)(2,1)}, u32[]{:S(2)}) copy-start(bf16[4096,512]{1,0:T(8,128)(2,1)} %param.17) | copy-start | bytes 12582916
  47.4 0.7 copy-start.3
  66.6 12.1 %all-to-all-start.1 = ((f32[4,2,4,128,32]{3,4,2,1,0:T(8,128)}), f32[4,2,4,128,32]{3,4,2,1,0:T(8,128)S(1)}, u32[]{:S(2)}, u32[]{:S(2)}) async-start(f32[4,2,4,128,32]{3,4,2,1,0:T(8,128)} %copy.38), calls=%async_computation.1 | async-start | bytes 1048576 | tf_op jit(solution)/shard_map/all_to_all | solution.py:152
  80.3 3.8 %copy-start.1 = (bf16[2,512]{1,0:T(2,128)(2,1)S(1)}, bf16[2,512]{1,0:T(2,128)(2,1)}, u32[]{:S(2)}) copy-start(bf16[2,512]{1,0:T(2,128)(2,1)} %param.21) | copy-start | bytes 6148
  80.3 3.8 %copy-start.4 = (bf16[2,512]{1,0:T(2,128)(2,1)S(1)}, bf16[2,512]{1,0:T(2,128)(2,1)}, u32[]{:S(2)}) copy-start(bf16[2,512]{1,0:T(2,128)(2,1)} %param.22) | copy-start | bytes 6148
  80.3 4.1 %copy-start.5 = (f32[2,4]{1,0:T(2,128)S(1)}, f32[2,4]{1,0:T(2,128)}, u32[]{:S(2)}) copy-start(f32[2,4]{1,0:T(2,128)} %param.24) | copy-start | bytes 100
  80.3 28.2 %all-to-all-start = ((f32[4,2,4,128,128]{4,3,2,1,0:T(8,128)}), f32[4,2,4,128,128]{4,3,2,1,0:T(8,128)S(1)}, u32[]{:S(2)}, u32[]{:S(2)}) async-start(f32[4,2,4,128,128]{4,3,2,1,0:T(8,128)} %broadcast_in_dim.51), calls=%async_computation | async-start | bytes 4194304 | tf_op jit(solution)/shard_map/all_to_all | solution.py:151
  108.5 5.1 %copy-start.2 = (bf16[2,4,32]{2,1,0:T(4,128)(2,1)S(1)}, bf16[2,4,32]{2,1,0:T(4,128)(2,1)}, u32[]{:S(2)}) copy-start(bf16[2,4,32]{2,1,0:T(4,128)(2,1)} %param.23) | copy-start | bytes 1540
  108.5 14.1 %copy-start.6 = (f32[32]{0:T(128)S(1)}, f32[32]{0:T(128)}, u32[]{:S(2)}) copy-start(f32[32]{0:T(128)} %param.25) | copy-start | bytes 388
Sparse Core Ops, SparseCore 0:
  9.6 31.8 all-gather.1
where the time goes:
time: 130 us
  waiting for transfers between devices  65 us (50%)
  matrix products  23.3 us (18%)
  between operations  14.4 us (11%)
  blocking collectives  8.86 us (7%)
  starting transfers between devices  7.41 us (6%)
  other arithmetic  5.62 us (4%)
  local copies, waits for them, and re-layouts  5.17 us (4%)
    all_gather x1, waiting for transfers between devices, local(): incoming = lax.all_gather(tokens, 'tp', axis=2, tiled=True)  31.8 us
    all_to_all x1, waiting for transfers between devices, local(): lax.all_to_all(carry_copies, 'sp', split_axis=0, concat_axis=0, tiled=True)  24.1 us
    psum x1, blocking collectives, local(): lax.psum(jnp.sum(read_raw * read_raw, axis=-1, keepdims=True), 'sp')  8.86 us
    all_to_all x1, waiting for transfers between devices, local(): lax.all_to_all(write_parts, 'sp', split_axis=0, concat_axis=0, tiled=True)  8.45 us
    dot_general x1, matrix products, local(): jnp.dot(flat_rows, key_matrix, preferred_element_type=jnp.float32)  4.21 us
    dot_general x6, matrix products, nilpotent_inverse(): jnp.einsum('...ij,...jk->...ik', result, powered, precision=exact_mode)  3.89 us
    all_to_all x1, starting transfers between devices, local(): lax.all_to_all(carry_copies, 'sp', split_axis=0, concat_axis=0, tiled=True)  3.74 us
    dot_general x4, matrix products, fold_step(): jnp.einsum('shij,shje->shie', block_map[0], current, precision=exact_mode)  3.69 us
  transfers between devices with their start and end apart: 3, of which 3 were waited for; matrix products, arithmetic and copies ran while one was open for 2% of the time, Pallas kernels for 0%

commit v1 on v0

--- a/solution.py
+++ b/solution.py
@@ -84,7 +84,7 @@
     strength_cols = lax.dynamic_slice_in_dim(gate_matrix, all_heads + first_head, local_heads, 1)
     gate_cols = jnp.concatenate([decay_cols, strength_cols], axis=1)
     row_count = sequences * positions
-    incoming = lax.all_gather(tokens, "tp", axis=2, tiled=True)
+    incoming = jnp.concatenate(lax.all_gather(tokens, "tp"), axis=2)
     span_width = incoming.shape[2]
     flat_rows = incoming.reshape(row_count, span_width)
     products = lax.optimization_barrier(

time: 130 us -> 137 us (1.054)
  local copies, waits for them, and re-layouts: 5.17 us -> 10.6 us
  other arithmetic: 5.62 us -> 9.28 us
  matrix products: 23.3 us -> 20.3 us
    add x4, other arithmetic: 0.13 us -> 3.76 us  [fold_step(): return (moved + block_map[1], None)]
    dot_general x1, matrix products: 4.21 us -> 1.24 us  [local(): jnp.dot(flat_rows, key_matrix, preferred_element_type=jnp.float32)]
    all_gather x0 -> x1, local copies, waits for them, and re-layouts: none -> 2.75 us  [local(): incoming = jnp.concatenate(lax.all_gather(tokens, 'tp'), axis=2)]
    unnamed x16 -> x19, local copies, waits for them, and re-layouts: 0.5 us -> 3.18 us
where the time goes in v1:
time: 137 us; the launch traced here: 136 us
  waiting for transfers between devices  65 us (47%)
  matrix products  20.3 us (15%)
  between operations  14.4 us (11%)
  local copies, waits for them, and re-layouts  10.6 us (8%)
  other arithmetic  9.28 us (7%)
  blocking collectives  8.86 us (6%)
  starting transfers between devices  7.43 us (5%)
    all_gather x1, waiting for transfers between devices, local(): incoming = jnp.concatenate(lax.all_gather(tokens, 'tp'), axis=2)  31.7 us
    all_to_all x1, waiting for transfers between devices, local(): lax.all_to_all(carry_copies, 'sp', split_axis=0, concat_axis=0, tiled=True)  24.1 us
    psum x1, blocking collectives, local(): lax.psum(jnp.sum(read_raw * read_raw, axis=-1, keepdims=True), 'sp')  8.86 us
    all_to_all x1, waiting for transfers between devices, local(): lax.all_to_all(write_parts, 'sp', split_axis=0, concat_axis=0, tiled=True)  8.44 us
    dot_general x6, matrix products, nilpotent_inverse(): jnp.einsum('...ij,...jk->...ik', result, powered, precision=exact_mode)  3.89 us
    add x4, other arithmetic, fold_step(): return (moved + block_map[1], None)  3.76 us
    all_to_all x1, starting transfers between devices, local(): lax.all_to_all(carry_copies, 'sp', split_axis=0, concat_axis=0, tiled=True)  3.75 us
    dot_general x4, matrix products, fold_step(): jnp.einsum('shij,shje->shie', block_map[0], current, precision=exact_mode)  3.69 us
  transfers between devices with their start and end apart: 3, of which 3 were waited for; matrix products, arithmetic and copies ran while one was open for 2% of the time, Pallas kernels for 0%

profile of v1, /device:TPU:0, one launch (start us, length us, event | category | flops | bytes accessed | tf_op | source)
XLA Modules:
  0.0 136.2 jit_solution(17599702234709158050)
XLA Ops:
  7.2 0.7 all-gather.3.cloned.1.call-update
  7.9 0.7 neg.14
  8.8 0.9 constant_dynamic-slice_fusion.2
  9.7 31.7 %all-gather.3.cloned.1.call-done = bf16[16,128,512]{2,1,0:T(8,128)(2,1)} async-done(((bf16[2,128,512]{2,1,0:T(8,128)(2,1)}), bf16[16,128,512]{2,1,0:T(8,128)(2,1)}) %all-gather.3.cloned.1.call-update) | async-done | bytes 2097168 | tf_op jit(solution)/shard_map/all_gather | solution.py:87
  41.5 2.8 %copy.28 = bf16[8,2,128,512]{3,0,2,1:T(8,128)(2,1)S(1)} copy(bf16[8,2,128,512]{3,2,1,0:T(8,128)(2,1)} %bitcast.104) | data formatting | bytes 4194304 | tf_op jit(solution)/shard_map/all_gather | solution.py:87
  44.2 0.9 copy.46
  45.2 1.3 copy-done.7
  46.4 1.2 fusion.52
  47.7 0.9 copy-done.8
  48.6 1.2 fusion.53
  49.9 0.6 convolution_bitcast_fusion
  50.7 1.1 reduce_window_sum.11
  51.8 0.2 slice_reduce_fusion
  52.1 0.2 reshape.112
  52.2 0.2 fusion.23
  52.5 0.2 bitcast_multiply_fusion
  52.8 0.2 reshape.114
  53.0 0.5 broadcast_multiply_fusion
  53.5 1.0 fusion.22
  54.5 0.6 fusion.54
  55.1 0.6 fusion.33
  55.7 0.6 fusion.55
  56.4 0.7 fusion.30
  57.0 0.6 fusion.56
  57.7 0.7 fusion.38
  58.4 0.1 fusion.37
  58.5 0.6 fusion.58
  59.1 0.6 fusion.57
  59.9 0.7 fusion.60
  60.5 0.7 fusion.59
  61.3 0.7 fusion.61
  61.9 0.7 fusion.24
  62.6 0.7 fusion.26
  63.3 4.5 %while.21 = (s32[]{:T(128)}, f32[2,4,128,256]{3,2,1,0:T(8,128)S(1)}, f32[2,2,4]{2,1,0:T(2,128)S(1)}, f32[2,2,4,64,128]{4,3,0,2,1:T(8,128)S(1)}, f32[2,2,4,64,128...) while((s32[]{:T(128)}, f32[2,4,128,256]{3,2,1,0:T(8,128)S(1)}, ...), condition=%wide.region_3.4_spmd, body=%wide.region_2.3_spmd.sunk | while | flops 403308544 | bytes 7602365 | solution.py:144
  63.5 0.7 fusion.107
  64.3 1.1 fusion.108
  65.4 0.3 multiply_add_fusion.3
  65.7 0.7 fusion.107
  66.4 1.1 fusion.108
  67.5 0.3 multiply_add_fusion.3
  67.8 0.3 copy.39
  68.2 0.8 copy.40
  69.0 3.6 %all-to-all-start.1 = ((f32[4,2,4,128,32]{3,4,2,1,0:T(8,128)}), f32[4,2,4,128,32]{3,4,2,1,0:T(8,128)S(1)}, u32[]{:S(2)}, u32[]{:S(2)}) async-start(f32[4,2,4,128,32]{3,4,2,1,0:T(8,128)} %copy.40), calls=%async_computation.1 | async-start | bytes 1048576 | tf_op jit(solution)/shard_map/all_to_all | solution.py:152
  72.7 8.4 %all-to-all-done.1 = f32[4,2,4,128,32]{3,4,2,1,0:T(8,128)S(1)} async-done(((f32[4,2,4,128,32]{3,4,2,1,0:T(8,128)}), f32[4,2,4,128,32]{3,4,2,1,0:T(8,128)S(1)}, u32[]{:S(2)}, u32[]{:S(2)}) %all-to-all-start.1) | async-done | bytes 524320 | tf_op jit(solution)/shard_map/all_to_all | solution.py:152
  81.2 1.6 %broadcast_in_dim.51 = f32[4,2,4,128,128]{4,3,2,1,0:T(8,128)} broadcast(f32[2,4,128,128]{3,2,1,0:T(8,128)S(1)} %slice.18), dimensions={1,2,3,4} | broadcast | bytes 2621440 | tf_op jit(solution)/shard_map/broadcast_in_dim | solution.py:147
  82.8 3.8 %all-to-all-start = ((f32[4,2,4,128,128]{4,3,2,1,0:T(8,128)}), f32[4,2,4,128,128]{4,3,2,1,0:T(8,128)S(1)}, u32[]{:S(2)}, u32[]{:S(2)}) async-start(f32[4,2,4,128,128]{4,3,2,1,0:T(8,128)} %broadcast_in_dim.51), calls=%async_computation | async-start | bytes 4194304 | tf_op jit(solution)/shard_map/all_to_all | solution.py:151
  86.6 0.1 multiply_reduce_fusion.2
  86.7 0.2 multiply_reduce_fusion.1
  86.9 24.1 %all-to-all-done = f32[4,2,4,128,128]{4,3,2,1,0:T(8,128)S(1)} async-done(((f32[4,2,4,128,128]{4,3,2,1,0:T(8,128)}), f32[4,2,4,128,128]{4,3,2,1,0:T(8,128)S(1)}, u32[]{:S(2)}, u32[]{:S(2)}) %all-to-all-start) | async-done | bytes 2097184 | tf_op jit(solution)/shard_map/all_to_all | solution.py:151
  111.0 7.5 %while.22 = (s32[]{:T(128)}, f32[2,4,128,32]{2,3,1,0:T(8,128)S(1)}, f32[4,2,4,128,128]{4,3,2,1,0:T(8,128)S(1)}, f32[4,2,4,128,32]{3,4,2,1,0:T(8,128)}, s32[]{:T(128)}, /*index=5*/s32[]{:T(128)}) while((s32[]{:T(128)}, f32[2,4,128,32]{2,3,1,0:T(8,128)S(1)}, f32[4,2,4,128,128]{4,3,2,1,0:T(8,128)S(1)}, ...), condition=%wide.region_5.6_spmd.clone, body=%wide.region_4.5_spmd.clone.sunk | while | flops 50397184 | bytes 1179735 | solution.py:161
  111.0 0.9 fusion.112
  111.9 0.9 bitcast_add_fusion.2
  112.8 0.9 fusion.112
  113.8 0.9 bitcast_add_fusion.2
  114.7 0.9 fusion.112
  115.6 0.9 bitcast_add_fusion.2
  116.6 0.9 fusion.112
  117.5 0.9 bitcast_add_fusion.2
  118.5 0.6 convert_element_type.39
  119.1 0.3 fusion.63
  119.4 0.2 fusion.62
  119.7 0.2 multiply_reduce_fusion
  119.8 8.9 %psum.7 = f32[2,4,1]{1,0,2:T(2,128)S(1)} all-reduce(f32[2,4,1]{1,0,2:T(2,128)S(1)} %bitcast.117), channel_id=1, replica_groups=mesh['sp'=4,'tp'=8] {'sp'}, use_global_device_ids=true, to_apply=%region_9.10 | all-reduce | flops 8 | bytes 64 | tf_op jit(solution)/shard_map/psum | solution.py:173
  128.7 0.7 multiply_convert_fusion
  (47 shorter events, 1.1 us)
Async XLA Ops:
  7.2 34.3 %all-gather.3.cloned.1.call-start = ((), (), s32[]{:S(2)}) async-start(), calls=%async_computation.2 | async-start | bytes 2359296 | tf_op jit(solution)/shard_map/all_gather | solution.py:87
  44.2 2.2 %copy-start.7 = (bf16[4096,512]{1,0:T(8,128)(2,1)S(1)}, bf16[4096,512]{1,0:T(8,128)(2,1)}, u32[]{:S(2)}) copy-start(bf16[4096,512]{1,0:T(8,128)(2,1)} %param.16) | copy-start | bytes 12582916
  46.4 2.2 %copy-start.8 = (bf16[4096,512]{1,0:T(8,128)(2,1)S(1)}, bf16[4096,512]{1,0:T(8,128)(2,1)}, u32[]{:S(2)}) copy-start(bf16[4096,512]{1,0:T(8,128)(2,1)} %param.17) | copy-start | bytes 12582916
  49.9 0.7 copy-start.3
  69.0 12.1 %all-to-all-start.1 = ((f32[4,2,4,128,32]{3,4,2,1,0:T(8,128)}), f32[4,2,4,128,32]{3,4,2,1,0:T(8,128)S(1)}, u32[]{:S(2)}, u32[]{:S(2)}) async-start(f32[4,2,4,128,32]{3,4,2,1,0:T(8,128)} %copy.40), calls=%async_computation.1 | async-start | bytes 1048576 | tf_op jit(solution)/shard_map/all_to_all | solution.py:152
  81.2 1.6 %copy-start = (f32[4,2,4,128,32]{3,4,2,1,0:T(8,128)}, f32[4,2,4,128,32]{3,4,2,1,0:T(8,128)S(1)}, u32[]{:S(2)}) copy-start(f32[4,2,4,128,32]{3,4,2,1,0:T(8,128)S(1)} %all-to-all-done.1) | copy-start | bytes 1572868
  82.8 3.8 %copy-start.1 = (bf16[2,512]{1,0:T(2,128)(2,1)S(1)}, bf16[2,512]{1,0:T(2,128)(2,1)}, u32[]{:S(2)}) copy-start(bf16[2,512]{1,0:T(2,128)(2,1)} %param.21) | copy-start | bytes 6148
  82.8 3.8 %copy-start.4 = (bf16[2,512]{1,0:T(2,128)(2,1)S(1)}, bf16[2,512]{1,0:T(2,128)(2,1)}, u32[]{:S(2)}) copy-start(bf16[2,512]{1,0:T(2,128)(2,1)} %param.22) | copy-start | bytes 6148
  82.8 4.1 %copy-start.5 = (f32[2,4]{1,0:T(2,128)S(1)}, f32[2,4]{1,0:T(2,128)}, u32[]{:S(2)}) copy-start(f32[2,4]{1,0:T(2,128)} %param.24) | copy-start | bytes 100
  82.8 28.2 %all-to-all-start = ((f32[4,2,4,128,128]{4,3,2,1,0:T(8,128)}), f32[4,2,4,128,128]{4,3,2,1,0:T(8,128)S(1)}, u32[]{:S(2)}, u32[]{:S(2)}) async-start(f32[4,2,4,128,128]{4,3,2,1,0:T(8,128)} %broadcast_in_dim.51), calls=%async_computation | async-start | bytes 4194304 | tf_op jit(solution)/shard_map/all_to_all | solution.py:151
  111.0 8.7 %copy-start.2 = (bf16[2,4,32]{2,1,0:T(4,128)(2,1)S(1)}, bf16[2,4,32]{2,1,0:T(4,128)(2,1)}, u32[]{:S(2)}) copy-start(bf16[2,4,32]{2,1,0:T(4,128)(2,1)} %param.23) | copy-start | bytes 1540
  111.0 17.7 %copy-start.6 = (f32[32]{0:T(128)S(1)}, f32[32]{0:T(128)}, u32[]{:S(2)}) copy-start(f32[32]{0:T(128)} %param.25) | copy-start | bytes 388
Sparse Core Ops, SparseCore 0:
  9.6 31.8 all-gather.2
